TPU v7x, 32 devices: a whole 2x2x4 slice. The times are simulated.
32 devices in a mesh: fs: 8 (over z, y), tp: 4 (over x, core).
Axes of the slice: x: 2, y: 2, z: 4, core: 2. Of those that a mesh axis runs over, the one named last changes fastest.
Arguments:
- tokens: bfloat16 [8192, 2048], P('fs', 'tp'), may hold values from -6 to 6
- mixer_gain: float32 [2048], replicated, may hold values from 0.1 to 1.9
- conv_taps: bfloat16 [3, 1024], replicated, may hold values from -3.5 to 3.5
- outer_weight: bfloat16 [2048, 1024], P('fs', 'tp'), may hold values from -0.125 to 0.125
- inner_weight: bfloat16 [2048, 1024], P('fs', 'tp'), may hold values from -0.125 to 0.125
- value_weight: bfloat16 [2048, 1024], P('fs', 'tp'), may hold values from -0.125 to 0.125
- merge_weight: bfloat16 [1024, 2048], P('tp', 'fs'), may hold values from -0.25 to 0.25
- merge_gain: float32 [2048], replicated, may hold values from 0.1 to 1.9
- channel_gain: float32 [2048], replicated, may hold values from 0.1 to 1.9
- gate_weight: bfloat16 [2048, 5632], P('fs', 'tp'), may hold values from -0.125 to 0.125
- up_weight: bfloat16 [2048, 5632], P('fs', 'tp'), may hold values from -0.125 to 0.125
- down_weight: bfloat16 [5632, 2048], P('tp', 'fs'), may hold values from -0.109375 to 0.109375
- output_gain: float32 [2048], replicated, may hold values from 0.1 to 1.9
Outputs:
- layer_out: bfloat16 [8192, 2048], P('fs', 'tp')
All inputs are finite; a program needn't handle non-finite values.
Results may differ from a plain program's by a relative error of at most 0.018.
Values may be sent and summed in bfloat16 or wider, within the bound.
A program may use at most 128 MiB of HBM per device.

v0:
```python
import jax
import jax.numpy as jnp
from jax import lax
from jax.sharding import PartitionSpec as P

HEAD_DIM = 128
EPS = 1e-06


def normalize(values):
    floats = values.astype(jnp.float32)
    return floats * lax.rsqrt(jnp.mean(floats * floats, axis=-1, keepdims=True) + EPS)


def rounded_term(partial_value):
    return lax.optimization_barrier(partial_value.astype(jnp.bfloat16)).astype(jnp.float32)


def finish_scatter(summed, residual, gain_row, squares):
    floats = summed.astype(jnp.float32)
    columns = floats.shape[1]
    factor = lax.rsqrt(squares / (columns * lax.axis_size("tp")) + EPS)
    own_gain = lax.dynamic_slice_in_dim(gain_row, lax.axis_index("tp") * columns, columns)
    return (residual.astype(jnp.float32) + floats * factor[:, None] * own_gain).astype(jnp.bfloat16)


def shards(
    tokens,
    mixer_gain,
    conv_taps,
    outer_weight,
    inner_weight,
    value_weight,
    merge_weight,
    merge_gain,
    channel_gain,
    gate_weight,
    up_weight,
    down_weight,
    output_gain,
):
    whole_tokens = lax.all_gather(tokens, "tp", axis=1, tiled=True)
    normed = (normalize(whole_tokens) * mixer_gain).astype(jnp.bfloat16)
    length = normed.shape[0]
    channels = outer_weight.shape[1]
    full_outer, full_inner, full_value = (
        lax.all_gather(outer_weight, "fs", axis=0, tiled=True),
        lax.all_gather(inner_weight, "fs", axis=0, tiled=True),
        lax.all_gather(value_weight, "fs", axis=0, tiled=True),
    )
    outer = jnp.dot(normed, full_outer, preferred_element_type=jnp.float32)
    inner = jnp.dot(normed, full_inner, preferred_element_type=jnp.float32)
    value = jnp.dot(normed, full_value, preferred_element_type=jnp.float32)
    own_taps = lax.dynamic_slice_in_dim(
        conv_taps, lax.axis_index("tp") * channels, channels, 1
    ).astype(jnp.float32)
    signal = inner * value
    padded = jnp.pad(signal, ((2, 0), (0, 0)))
    conv = (
        own_taps[0] * padded[:length]
        + own_taps[1] * padded[1 : length + 1]
        + own_taps[2] * padded[2:]
    )
    gated = (outer * conv).reshape(length, channels // HEAD_DIM, HEAD_DIM)
    mixed = normalize(gated).reshape(length, channels).astype(jnp.bfloat16)
    merged_part = jnp.dot(
        mixed,
        lax.all_gather(merge_weight, "fs", axis=1, tiled=True),
        preferred_element_type=jnp.float32,
    )
    merged = lax.psum(rounded_term(merged_part).astype(jnp.bfloat16), "tp")
    first_full = (whole_tokens.astype(jnp.float32) + normalize(merged) * merge_gain).astype(
        jnp.bfloat16
    )
    width = tokens.shape[1]
    first = lax.dynamic_slice_in_dim(first_full, lax.axis_index("tp") * width, width, 1)
    normed2 = (normalize(first_full) * channel_gain).astype(jnp.bfloat16)
    full_gate, full_up = (
        lax.all_gather(gate_weight, "fs", axis=0, tiled=True),
        lax.all_gather(up_weight, "fs", axis=0, tiled=True),
    )
    gate = jnp.dot(normed2, full_gate, preferred_element_type=jnp.float32)
    upward = jnp.dot(normed2, full_up, preferred_element_type=jnp.float32)
    hidden = (jax.nn.silu(gate) * upward).astype(jnp.bfloat16)
    down_part = jnp.dot(
        hidden,
        lax.all_gather(down_weight, "fs", axis=1, tiled=True),
        preferred_element_type=jnp.float32,
    )
    down = lax.psum_scatter(
        rounded_term(down_part).astype(jnp.bfloat16), "tp", scatter_dimension=1, tiled=True
    )
    down_float = down.astype(jnp.float32)
    down_squares = lax.psum(jnp.sum(down_float * down_float, axis=1), "tp")
    return finish_scatter(down, first, output_gain, down_squares)


def solution(mesh):
    return jax.shard_map(
        shards,
        mesh=mesh,
        in_specs=(
            P("fs", "tp"),
            P(),
            P(),
            P("fs", "tp"),
            P("fs", "tp"),
            P("fs", "tp"),
            P("tp", "fs"),
            P(),
            P(),
            P("fs", "tp"),
            P("fs", "tp"),
            P("tp", "fs"),
            P(),
        ),
        out_specs=P("fs", "tp"),
        check_vma=False,
    )
```

profile of v0, /device:TPU:0, one launch (start us, length us, event | category | flops | bytes accessed | tf_op | source)
XLA Modules:
  0.0 661.4 jit_solution(1043669761443059637)
XLA Ops:
  6.5 0.7 all-gather.9.cloned.1.call-update
  7.3 0.7 all-gather.13.cloned.1.call-update
  8.1 0.7 all-gather.15.cloned.1.call-update
  8.8 0.5 all-gather.11.cloned.1.call-update
  9.4 0.5 all-gather.17.cloned.1.call-update
  10.0 0.7 dynamic-slice_convert_fusion
  10.7 35.5 %all-gather.9.cloned.1.call-done = bf16[1024,2048]{1,0:T(8,128)(2,1)} async-done(((bf16[1024,512]{1,0:T(8,128)(2,1)}), bf16[1024,2048]{1,0:T(8,128)(2,1)}) %all-gather.9.cloned.1.call-update) | async-done | bytes 4194320 | tf_op jit(solution)/shard_map/all_gather | solution.py:42
  46.1 3.1 fusion.5
  49.2 39.4 %all-gather.13.cloned.1.call-done = bf16[2048,256]{1,0:T(8,128)(2,1)} async-done(((bf16[256,256]{1,0:T(8,128)(2,1)}), bf16[2048,256]{1,0:T(8,128)(2,1)}) %all-gather.13.cloned.1.call-update) | async-done | bytes 1048592 | tf_op jit(solution)/shard_map/all_gather | solution.py:48
  88.5 4.0 fusion.22
  92.5 37.2 %all-gather.15.cloned.1.call-done = bf16[2048,256]{1,0:T(8,128)(2,1)} async-done(((bf16[256,256]{1,0:T(8,128)(2,1)}), bf16[2048,256]{1,0:T(8,128)(2,1)}) %all-gather.15.cloned.1.call-update) | async-done | bytes 1048592 | tf_op jit(solution)/shard_map/all_gather | solution.py:49
  129.7 4.0 convolution_multiply_fusion
  133.7 37.0 %all-gather.11.cloned.1.call-done = bf16[2048,256]{1,0:T(8,128)(2,1)} async-done(((bf16[256,256]{1,0:T(8,128)(2,1)}), bf16[2048,256]{1,0:T(8,128)(2,1)}) %all-gather.11.cloned.1.call-update) | async-done | bytes 1048592 | tf_op jit(solution)/shard_map/all_gather | solution.py:47
  170.7 4.4 bitcast_reduce_fusion
  175.2 35.5 %all-gather.17.cloned.1.call-done = bf16[256,2048]{1,0:T(8,128)(2,1)} async-done(((bf16[256,256]{1,0:T(8,128)(2,1)}), bf16[256,2048]{1,0:T(8,128)(2,1)}) %all-gather.17.cloned.1.call-update) | async-done | bytes 1048592 | tf_op jit(solution)/shard_map/all_gather | solution.py:68
  210.7 4.6 convolution_convert_fusion.1
  215.4 0.7 all-gather.19.cloned.1.call-update
  216.1 0.7 all-gather.21.cloned.1.call-update
  216.9 0.7 all-gather.23.cloned.1.call-update
  217.8 82.2 %all-reduce.3.cloned.1.call-done = bf16[1024,2048]{1,0:T(8,128)(2,1)} async-done(((bf16[1024,2048]{1,0:T(8,128)(2,1)}), bf16[1024,2048]{1,0:T(8,128)(2,1)}) %all-reduce.3.cloned.1.call-update) | async-done | bytes 4194320 | tf_op jit(solution)/shard_map/psum | solution.py:71
  300.0 3.2 fusion
  303.4 5.3 fusion.2
  308.8 85.9 %all-gather.19.cloned.1.call-done = bf16[2048,1408]{1,0:T(8,128)(2,1)} async-done(((bf16[256,1408]{1,0:T(8,128)(2,1)}), bf16[2048,1408]{1,0:T(8,128)(2,1)}) %all-gather.19.cloned.1.call-update) | async-done | bytes 5767184 | tf_op jit(solution)/shard_map/all_gather | solution.py:79
  394.6 12.0 %fusion.14 = f32[1024,1408]{1,0:T(8,128)} fusion(bf16[2048,1408]{1,0:T(8,128)(2,1)} %all-gather.19.cloned.1.call-done, bf16[1024,2048]{1,0:T(8,128)(2,1)} %get-tuple-element.6, f32[2048]{0:T(1024)S(1)} %copy-done.3, f32[1024]{0:T(1024)S(1)} %add_rsqrt_fusion.2), kind=kOutput, calls=%fused_computation.27 | convolution fusion | flops 5913968640 | bytes 15740928 | tf_op jit(solution)/shard_map/dot_general | solution.py:82
  406.6 80.7 %all-gather.21.cloned.1.call-done = bf16[2048,1408]{1,0:T(8,128)(2,1)} async-done(((bf16[256,1408]{1,0:T(8,128)(2,1)}), bf16[2048,1408]{1,0:T(8,128)(2,1)}) %all-gather.21.cloned.1.call-update) | async-done | bytes 5767184 | tf_op jit(solution)/shard_map/all_gather | solution.py:80
  487.3 93.4 %all-gather.23.cloned.1.call-done = bf16[1408,2048]{1,0:T(8,128)(2,1)} async-done(((bf16[1408,256]{1,0:T(8,128)(2,1)}), bf16[1408,2048]{1,0:T(8,128)(2,1)}) %all-gather.23.cloned.1.call-update) | async-done | bytes 5767184 | tf_op jit(solution)/shard_map/all_gather | solution.py:87
  580.7 20.8 %convolution_convert_fusion = bf16[1024,2048]{1,0:T(8,128)(2,1)} fusion(bf16[1408,2048]{1,0:T(8,128)(2,1)} %all-gather.23.cloned.1.call-done, f32[1024,1408]{1,0:T(8,128)} %fusion.14, bf16[2048,1408]{1,0:T(8,128)(2,1)} %all-gather.21.cloned.1.call-done, bf16[1024,2048]{1,0:T(8,128)(2,1)} %get-tuple-element.6, f32[2048]{0:T(1024)S(1)} %copy-done.3, ...), kind=kOutput, calls=%fused_computation.17 | convolution fusion | flops 11830296576 | bytes 25702400 | tf_op jit(solution)/shard_map/dot_general | solution.py:85
  601.6 0.8 dynamic_slice.11
  602.3 42.0 %reduce-scatter.2.cloned.1.call-done = bf16[1024,512]{1,0:T(8,128)(2,1)} async-done(((bf16[1024,2048]{1,0:T(8,128)(2,1)}), bf16[1024,512]{1,0:T(8,128)(2,1)}) %reduce-scatter.2.cloned.1.call-update) | async-done | bytes 1048592 | tf_op jit(solution)/shard_map/reduce_scatter | solution.py:90
  644.3 1.5 fusion.9
  645.8 5.8 psum.15
  651.6 3.0 fusion.12
  (27 shorter events, 0.9 us)
Async XLA Ops:
  6.5 82.0 %copy-start.2 = (f32[2048]{0:T(1024)S(1)}, f32[2048]{0:T(1024)}, u32[]{:S(2)}) copy-start(f32[2048]{0:T(1024)} %param.14) | copy-start | bytes 24580
  6.5 39.6 %all-gather.9.cloned.1.call-start = ((), (), s32[]{:S(2)}) async-start(), calls=%async_computation.1 | async-start | bytes 5242880 | tf_op jit(solution)/shard_map/all_gather | solution.py:42
  7.3 81.3 %all-gather.13.cloned.1.call-start = ((), (), s32[]{:S(2)}) async-start(), calls=%async_computation.3 | async-start | bytes 1179648 | tf_op jit(solution)/shard_map/all_gather | solution.py:48
  8.0 121.7 %all-gather.15.cloned.1.call-start = ((), (), s32[]{:S(2)}) async-start(), calls=%async_computation.4 | async-start | bytes 1179648 | tf_op jit(solution)/shard_map/all_gather | solution.py:49
  8.7 162.0 %all-gather.11.cloned.1.call-start = ((), (), s32[]{:S(2)}) async-start(), calls=%async_computation.2 | async-start | bytes 1179648 | tf_op jit(solution)/shard_map/all_gather | solution.py:47
  9.3 201.4 %all-gather.17.cloned.1.call-start = ((), (), s32[]{:S(2)}) async-start(), calls=%async_computation.5 | async-start | bytes 1179648 | tf_op jit(solution)/shard_map/all_gather | solution.py:68
  9.9 290.1 %all-reduce.3.cloned.1.call-start = ((), (), s32[]{:S(2)}) async-start(), calls=%async_computation.6 | async-start | bytes 8388608 | tf_op jit(solution)/shard_map/psum | solution.py:71
  215.3 87.9 %copy-start.1 = (f32[2048]{0:T(1024)S(1)}, f32[2048]{0:T(1024)}, u32[]{:S(2)}) copy-start(f32[2048]{0:T(1024)} %param.20) | copy-start | bytes 24580
  215.3 179.3 %all-gather.19.cloned.1.call-start = ((), (), s32[]{:S(2)}) async-start(), calls=%async_computation.7 | async-start | bytes 6488064 | tf_op jit(solution)/shard_map/all_gather | solution.py:79
  216.1 271.3 %all-gather.21.cloned.1.call-start = ((), (), s32[]{:S(2)}) async-start(), calls=%async_computation.8 | async-start | bytes 6488064 | tf_op jit(solution)/shard_map/all_gather | solution.py:80
  216.8 363.9 %all-gather.23.cloned.1.call-start = ((), (), s32[]{:S(2)}) async-start(), calls=%async_computation.9 | async-start | bytes 6488064 | tf_op jit(solution)/shard_map/all_gather | solution.py:87
  217.5 426.8 %reduce-scatter.2.cloned.1.call-start = ((), (), s32[]{:S(2)}) async-start(), calls=%async_computation.10 | async-start | bytes 5242880 | tf_op jit(solution)/shard_map/reduce_scatter | solution.py:90
  300.0 3.4 copy-start
  303.4 91.2 %copy-start.3 = (f32[2048]{0:T(1024)S(1)}, f32[2048]{0:T(1024)}, u32[]{:S(2)}) copy-start(f32[2048]{0:T(1024)} %param.21) | copy-start | bytes 24580
Sparse Core Ops, SparseCore 0:
  8.9 37.1 all-gather.8
  48.2 40.2 all-gather.12
  90.7 38.9 all-gather.14
  131.7 38.9 all-gather.10
  172.6 38.0 all-gather.16
  215.4 84.4 all-reduce.2
  302.1 92.4 all-gather.18
  396.8 90.4 all-gather.20
  489.4 91.2 all-gather.22
  601.7 42.5 reduce-scatter.1
where the time goes:
time: 662 us; the launch traced here: 661 us
  waiting for transfers between devices  574 us (87%)
  matrix products  49.7 us (8%)
  other arithmetic  16.9 us (3%)
  between operations  13.6 us (2%)
    all_gather x1, waiting for transfers between devices, shards(): lax.all_gather(down_weight, 'fs', axis=1, tiled=True)  93.4 us
    all_gather x1, waiting for transfers between devices, shards(): lax.all_gather(gate_weight, 'fs', axis=0, tiled=True)  85.9 us
    psum x1, waiting for transfers between devices, shards(): merged = lax.psum(rounded_term(merged_part).astype(jnp.bfloat16), 'tp')  82.2 us
    all_gather x1, waiting for transfers between devices, shards(): lax.all_gather(up_weight, 'fs', axis=0, tiled=True)  80.7 us
    reduce_scatter x1, waiting for transfers between devices, shards(): lax.psum_scatter(rounded_term(down_part).astype(jnp.bfloat16), 'tp', scat...  42 us
    all_gather x1, waiting for transfers between devices, shards(): lax.all_gather(inner_weight, 'fs', axis=0, tiled=True)  39.4 us
    all_gather x1, waiting for transfers between devices, shards(): lax.all_gather(value_weight, 'fs', axis=0, tiled=True)  37.2 us
    all_gather x1, waiting for transfers between devices, shards(): lax.all_gather(outer_weight, 'fs', axis=0, tiled=True)  37 us
  transfers between devices with their start and end apart: 10, of which 10 were waited for; matrix products, arithmetic and copies ran while one was open for 6% of the time, Pallas kernels for 0%

commit v1 on v0

--- a/solution.py
+++ b/solution.py
@@ -68,7 +68,7 @@
         lax.all_gather(merge_weight, "fs", axis=1, tiled=True),
         preferred_element_type=jnp.float32,
     )
-    merged = lax.psum(rounded_term(merged_part).astype(jnp.bfloat16), "tp")
+    merged = jnp.sum(lax.all_gather(rounded_term(merged_part).astype(jnp.bfloat16), "tp"), axis=0)
     first_full = (whole_tokens.astype(jnp.float32) + normalize(merged) * merge_gain).astype(
         jnp.bfloat16
     )

time: 662 us -> 682 us (1.030)
  other arithmetic: 16.9 us -> 29.2 us
  waiting for transfers between devices: 574 us -> 582 us
    all_gather x0 -> x1, waiting for transfers between devices: none -> 103 us  [shards(): lax.all_gather(rounded_term(merged_part).astype(jnp.bfloat16), 'tp')]
    psum x1 -> x0, waiting for transfers between devices: 82.2 us -> none  [shards(): merged = lax.psum(rounded_term(merged_part).astype(jnp.bfloat16), 'tp')]
    all_gather x1, waiting for transfers between devices: 85.9 us -> 73.5 us  [shards(): lax.all_gather(gate_weight, 'fs', axis=0, tiled=True)]
    reduce_sum x0 -> x1, other arithmetic: none -> 12.1 us  [shards(): jnp.sum(lax.all_gather(rounded_term(merged_part).astype(jnp.bfloat16), 't...]
  transfers between devices with their start and end apart: 10 -> 10, of which waited for: 10 -> 10; matrix products, arithmetic and copies ran while one was open for 6% -> 7% of each run, Pallas kernels for 0% -> 0%
where the time goes in v1:
time: 682 us
  waiting for transfers between devices  582 us (85%)
  matrix products  49.7 us (7%)
  other arithmetic  29.2 us (4%)
  between operations  13.6 us (2%)
    all_gather x1, waiting for transfers between devices, shards(): lax.all_gather(rounded_term(merged_part).astype(jnp.bfloat16), 'tp')  103 us
    all_gather x1, waiting for transfers between devices, shards(): lax.all_gather(down_weight, 'fs', axis=1, tiled=True)  93.4 us
    all_gather x1, waiting for transfers between devices, shards(): lax.all_gather(up_weight, 'fs', axis=0, tiled=True)  80.8 us
    all_gather x1, waiting for transfers between devices, shards(): lax.all_gather(gate_weight, 'fs', axis=0, tiled=True)  73.5 us
    reduce_scatter x1, waiting for transfers between devices, shards(): lax.psum_scatter(rounded_term(down_part).astype(jnp.bfloat16), 'tp', scat...  42 us
    all_gather x1, waiting for transfers between devices, shards(): lax.all_gather(inner_weight, 'fs', axis=0, tiled=True)  39.4 us
    all_gather x1, waiting for transfers between devices, shards(): lax.all_gather(value_weight, 'fs', axis=0, tiled=True)  37.2 us
    all_gather x1, waiting for transfers between devices, shards(): lax.all_gather(outer_weight, 'fs', axis=0, tiled=True)  37 us
  transfers between devices with their start and end apart: 10, of which 10 were waited for; matrix products, arithmetic and copies ran while one was open for 7% of the time, Pallas kernels for 0%

profile of v1, /device:TPU:0, one launch (start us, length us, event | category | flops | bytes accessed | tf_op | source)
XLA Modules:
  0.0 681.7 jit_solution(1234677315943103706)
XLA Ops:
  6.5 0.7 all-gather.11.cloned.1.call-update
  7.3 0.7 all-gather.15.cloned.1.call-update
  8.1 0.7 all-gather.17.cloned.1.call-update
  9.4 0.5 all-gather.19.cloned.1.call-update
  10.0 0.7 dynamic-slice_convert_fusion
  10.7 35.5 %all-gather.11.cloned.1.call-done = bf16[1024,2048]{1,0:T(8,128)(2,1)} async-done(((bf16[1024,512]{1,0:T(8,128)(2,1)}), bf16[1024,2048]{1,0:T(8,128)(2,1)}) %all-gather.11.cloned.1.call-update) | async-done | bytes 4194320 | tf_op jit(solution)/shard_map/all_gather | solution.py:42
  46.1 3.1 fusion.5
  49.2 39.4 %all-gather.15.cloned.1.call-done = bf16[2048,256]{1,0:T(8,128)(2,1)} async-done(((bf16[256,256]{1,0:T(8,128)(2,1)}), bf16[2048,256]{1,0:T(8,128)(2,1)}) %all-gather.15.cloned.1.call-update) | async-done | bytes 1048592 | tf_op jit(solution)/shard_map/all_gather | solution.py:48
  88.5 4.0 fusion.22
  92.5 37.2 %all-gather.17.cloned.1.call-done = bf16[2048,256]{1,0:T(8,128)(2,1)} async-done(((bf16[256,256]{1,0:T(8,128)(2,1)}), bf16[2048,256]{1,0:T(8,128)(2,1)}) %all-gather.17.cloned.1.call-update) | async-done | bytes 1048592 | tf_op jit(solution)/shard_map/all_gather | solution.py:49
  129.7 4.0 convolution_multiply_fusion
  133.7 37.0 %all-gather.13.cloned.1.call-done = bf16[2048,256]{1,0:T(8,128)(2,1)} async-done(((bf16[256,256]{1,0:T(8,128)(2,1)}), bf16[2048,256]{1,0:T(8,128)(2,1)}) %all-gather.13.cloned.1.call-update) | async-done | bytes 1048592 | tf_op jit(solution)/shard_map/all_gather | solution.py:47
  170.7 4.4 bitcast_reduce_fusion
  175.2 35.5 %all-gather.19.cloned.1.call-done = bf16[256,2048]{1,0:T(8,128)(2,1)} async-done(((bf16[256,256]{1,0:T(8,128)(2,1)}), bf16[256,2048]{1,0:T(8,128)(2,1)}) %all-gather.19.cloned.1.call-update) | async-done | bytes 1048592 | tf_op jit(solution)/shard_map/all_gather | solution.py:68
  210.7 4.5 convolution_convert_fusion.1
  215.3 0.7 all-gather.21.cloned.1.call-update
  216.1 0.7 all-gather.23.cloned.1.call-update
  216.8 0.7 all-gather.25.cloned.1.call-update
  217.7 102.6 %all-gather.27.cloned.1.call-done = bf16[4096,2048]{1,0:T(8,128)(2,1)} async-done(((bf16[1024,2048]{1,0:T(8,128)(2,1)}), bf16[4096,2048]{1,0:T(8,128)(2,1)}) %all-gather.27.cloned.1.call-update) | async-done | bytes 16777232 | tf_op jit(solution)/shard_map/all_gather | solution.py:71
  320.3 12.1 %reduce_sum.59 = bf16[1024,2048]{1,0:T(8,128)(2,1)} reduce(bf16[4,1024,2048]{2,1,0:T(8,128)(2,1)} %bitcast.23, bf16[]{:T(256)} %constant.32.clone.1), dimensions={0}, to_apply=%region_2.3 | reduce | flops 6291456 | bytes 20971522 | tf_op jit(solution)/shard_map/reduce_sum | solution.py:71
  332.4 3.2 fusion
  335.9 5.5 fusion.2
  341.4 73.5 %all-gather.21.cloned.1.call-done = bf16[2048,1408]{1,0:T(8,128)(2,1)} async-done(((bf16[256,1408]{1,0:T(8,128)(2,1)}), bf16[2048,1408]{1,0:T(8,128)(2,1)}) %all-gather.21.cloned.1.call-update) | async-done | bytes 5767184 | tf_op jit(solution)/shard_map/all_gather | solution.py:79
  414.9 11.9 %fusion.14 = f32[1024,1408]{1,0:T(8,128)} fusion(bf16[2048,1408]{1,0:T(8,128)(2,1)} %all-gather.21.cloned.1.call-done, bf16[1024,2048]{1,0:T(8,128)(2,1)} %get-tuple-element.6, f32[2048]{0:T(1024)S(1)} %copy-done.3, f32[1024]{0:T(1024)S(1)} %add_rsqrt_fusion.2), kind=kOutput, calls=%fused_computation.27 | convolution fusion | flops 5913968640 | bytes 15740928 | tf_op jit(solution)/shard_map/dot_general | solution.py:82
  426.8 80.8 %all-gather.23.cloned.1.call-done = bf16[2048,1408]{1,0:T(8,128)(2,1)} async-done(((bf16[256,1408]{1,0:T(8,128)(2,1)}), bf16[2048,1408]{1,0:T(8,128)(2,1)}) %all-gather.23.cloned.1.call-update) | async-done | bytes 5767184 | tf_op jit(solution)/shard_map/all_gather | solution.py:80
  507.6 93.4 %all-gather.25.cloned.1.call-done = bf16[1408,2048]{1,0:T(8,128)(2,1)} async-done(((bf16[1408,256]{1,0:T(8,128)(2,1)}), bf16[1408,2048]{1,0:T(8,128)(2,1)}) %all-gather.25.cloned.1.call-update) | async-done | bytes 5767184 | tf_op jit(solution)/shard_map/all_gather | solution.py:87
  601.0 20.9 %convolution_convert_fusion = bf16[1024,2048]{1,0:T(8,128)(2,1)} fusion(bf16[1408,2048]{1,0:T(8,128)(2,1)} %all-gather.25.cloned.1.call-done, f32[1024,1408]{1,0:T(8,128)} %fusion.14, bf16[2048,1408]{1,0:T(8,128)(2,1)} %all-gather.23.cloned.1.call-done, bf16[1024,2048]{1,0:T(8,128)(2,1)} %get-tuple-element.6, f32[2048]{0:T(1024)S(1)} %copy-done.3, ...), kind=kOutput, calls=%fused_computation.17 | convolution fusion | flops 11830296576 | bytes 25702400 | tf_op jit(solution)/shard_map/dot_general | solution.py:85
  621.9 0.8 dynamic_slice.11
  622.6 42.0 %reduce-scatter.2.cloned.1.call-done = bf16[1024,512]{1,0:T(8,128)(2,1)} async-done(((bf16[1024,2048]{1,0:T(8,128)(2,1)}), bf16[1024,512]{1,0:T(8,128)(2,1)}) %reduce-scatter.2.cloned.1.call-update) | async-done | bytes 1048592 | tf_op jit(solution)/shard_map/reduce_scatter | solution.py:90
  664.6 1.5 fusion.9
  666.1 5.8 psum.7
  671.9 3.0 fusion.12
  (28 shorter events, 1.4 us)
Async XLA Ops:
  6.5 82.0 %copy-start.2 = (f32[2048]{0:T(1024)S(1)}, f32[2048]{0:T(1024)}, u32[]{:S(2)}) copy-start(f32[2048]{0:T(1024)} %param.14) | copy-start | bytes 24580
  6.5 39.6 %all-gather.11.cloned.1.call-start = ((), (), s32[]{:S(2)}) async-start(), calls=%async_computation.1 | async-start | bytes 5242880 | tf_op jit(solution)/shard_map/all_gather | solution.py:42
  7.3 81.3 %all-gather.15.cloned.1.call-start = ((), (), s32[]{:S(2)}) async-start(), calls=%async_computation.3 | async-start | bytes 1179648 | tf_op jit(solution)/shard_map/all_gather | solution.py:48
  8.0 121.7 %all-gather.17.cloned.1.call-start = ((), (), s32[]{:S(2)}) async-start(), calls=%async_computation.4 | async-start | bytes 1179648 | tf_op jit(solution)/shard_map/all_gather | solution.py:49
  8.7 162.0 %all-gather.13.cloned.1.call-start = ((), (), s32[]{:S(2)}) async-start(), calls=%async_computation.2 | async-start | bytes 1179648 | tf_op jit(solution)/shard_map/all_gather | solution.py:47
  9.3 201.4 %all-gather.19.cloned.1.call-start = ((), (), s32[]{:S(2)}) async-start(), calls=%async_computation.5 | async-start | bytes 1179648 | tf_op jit(solution)/shard_map/all_gather | solution.py:68
  9.9 310.4 %all-gather.27.cloned.1.call-start = ((), (), s32[]{:S(2)}) async-start(), calls=%async_computation.10 | async-start | bytes 20971520 | tf_op jit(solution)/shard_map/all_gather | solution.py:71
  215.3 199.6 %all-gather.21.cloned.1.call-start = ((), (), s32[]{:S(2)}) async-start(), calls=%async_computation.6 | async-start | bytes 6488064 | tf_op jit(solution)/shard_map/all_gather | solution.py:79
  216.0 291.5 %all-gather.23.cloned.1.call-start = ((), (), s32[]{:S(2)}) async-start(), calls=%async_computation.7 | async-start | bytes 6488064 | tf_op jit(solution)/shard_map/all_gather | solution.py:80
  216.8 384.2 %all-gather.25.cloned.1.call-start = ((), (), s32[]{:S(2)}) async-start(), calls=%async_computation.8 | async-start | bytes 6488064 | tf_op jit(solution)/shard_map/all_gather | solution.py:87
  217.5 447.1 %reduce-scatter.2.cloned.1.call-start = ((), (), s32[]{:S(2)}) async-start(), calls=%async_computation.9 | async-start | bytes 5242880 | tf_op jit(solution)/shard_map/reduce_scatter | solution.py:90
  320.3 15.3 %copy-start.1 = (f32[2048]{0:T(1024)S(1)}, f32[2048]{0:T(1024)}, u32[]{:S(2)}) copy-start(f32[2048]{0:T(1024)} %param.20) | copy-start | bytes 24580
  332.4 3.4 copy-start
  335.9 79.0 %copy-start.3 = (f32[2048]{0:T(1024)S(1)}, f32[2048]{0:T(1024)}, u32[]{:S(2)}) copy-start(f32[2048]{0:T(1024)} %param.21) | copy-start | bytes 24580
Sparse Core Ops, SparseCore 0:
  8.9 37.1 all-gather.10
  48.2 40.2 all-gather.14
  90.7 38.9 all-gather.16
  131.7 38.9 all-gather.12
  172.6 38.0 all-gather.18
  215.4 104.8 all-gather.26
  322.5 92.3 all-gather.20
  417.0 90.4 all-gather.22
  509.6 91.2 all-gather.24
  622.0 42.5 reduce-scatter.1
